TPU v7x, 32 devices: a whole 2x2x4 slice. The times are simulated.
32 devices in a mesh: kv: 8 (over z, y), tp: 4 (over x, core).
Axes of the slice: x: 2, y: 2, z: 4, core: 2. Of those that a mesh axis runs over, the one named last changes fastest.
Arguments:
- inputs: bfloat16 [4096, 2048], P('kv'), may hold values from -128 to 128
- w_query: bfloat16 [2048, 2048], P(None, 'tp'), may hold values from -0.125 to 0.125
- w_key: bfloat16 [2048, 1024], P(None, 'tp'), may hold values from -0.125 to 0.125
- w_value: bfloat16 [2048, 1024], P(None, 'tp'), may hold values from -0.125 to 0.125
- w_out: bfloat16 [2048, 2048], P(None, 'tp'), may hold values from -0.125 to 0.125
- chosen: int32 [128, 8], P('kv'), may hold values from -1 to 127, as said below
Outputs:
- mixed: bfloat16 [4096, 2048], P('kv', 'tp')
- log_total: float32 [16, 4096], P('tp', 'kv')
Inputs may be any that keep to these rules, and one draw needn't show every extreme that they name: `chosen`: row i has entry 0 equal to i. Rows 16 * r to 16 * r + 15 belong to index r of kv. For k from 1 to 7, entry k of these rows is -1 or one and the same block held by index r - d, with d = 1 + (k - 1) * 1; it is -1 in all of them where r - d is negative, and the last of these rows lists every such block that exists.
All inputs are finite; a program needn't handle non-finite values.
Results may differ from a plain program's by a relative error of at most 0.015.
Values may be sent and summed in bfloat16 or wider, within the bound.
A program may use at most 192 MiB of HBM per device.

v0:
```python
import functools

import jax
import jax.numpy as jnp
import numpy as np
from jax import lax
from jax.experimental import pallas as pl
from jax.experimental.pallas import tpu as pltpu
from jax.sharding import PartitionSpec as P

HD = 128
BLK = 32
TILE = 128
MESH = pl.DeviceIdType.MESH
F32 = jnp.float32
BF16 = jnp.bfloat16


def iota(shape, dim):
    return lax.broadcasted_iota(jnp.int32, shape, dim)


def kernel(
    peers, tp, x_hbm, wq_hbm, wk_hbm, wv_hbm, wo_hbm, chosen_hbm,
    out_hbm, log_hbm,
    x, wq, wk, wv, wo, chosen, cosine, sine, kv, q, request, pick, stage, far, bias, gathered, acc, out, log_total,
    load_sem, store_sem, req_send, req_recv, far_send, far_recv,
    ring_send, ring_recv, side_send, side_recv, pass_send, pass_recv,
):
    tokens = x.shape[0]
    heads = wq.shape[1] // HD
    kv_heads = wk.shape[1] // HD
    group = heads // kv_heads
    blocks = tokens // BLK
    count = chosen.shape[0] - 1
    reaches = [1 + k * (peers - 2) // (count - 1) for k in range(count)]
    chips = tp // 2
    tiles = tokens // TILE
    me = lax.axis_index("kv")
    lane = lax.axis_index("tp")
    chip, core = lane // 2, lane % 2
    partner = chip * 2 + 1 - core
    scale = HD ** -0.5

    loads = [
        pltpu.make_async_copy(s, d, load_sem.at[i])
        for i, (s, d) in enumerate(
            [(chosen_hbm, chosen), (x_hbm, x), (wk_hbm, wk), (wv_hbm, wv),
             (wq_hbm, wq), (wo_hbm, wo)]
        )
    ]

    barrier = pltpu.get_barrier_semaphore()
    expected = jnp.int32(chips)
    for d in reaches:
        @pl.when(me >= d)
        def _():
            pl.semaphore_signal(barrier, inc=1, device_id=(me - d, lane), device_id_type=MESH)

        @pl.when(me + d < peers)
        def _():
            pl.semaphore_signal(barrier, inc=1, device_id=(me + d, lane), device_id_type=MESH)

        expected = expected + jnp.where(me >= d, 1, 0) + jnp.where(me + d < peers, 1, 0)
    pl.semaphore_signal(barrier, inc=1, device_id=(me, partner), device_id_type=MESH)
    for step in range(1, chips):
        other = lax.rem(chip + step, chips) * 2 + core
        pl.semaphore_signal(barrier, inc=1, device_id=(me, other), device_id_type=MESH)
    for load in loads[:4]:
        load.start()

    def request_copy(k):
        return pltpu.make_async_remote_copy(
            src_ref=chosen, dst_ref=request.at[k], send_sem=req_send.at[k],
            recv_sem=req_recv.at[k], device_id=(me - reaches[k], lane), device_id_type=MESH,
        )

    def far_copy(k):
        rows = pl.ds(k * BLK, BLK)
        return pltpu.make_async_remote_copy(
            src_ref=stage.at[rows], dst_ref=far.at[rows], send_sem=far_send.at[k],
            recv_sem=far_recv.at[k], device_id=(me + reaches[k], lane), device_id_type=MESH,
        )

    half = HD // 2
    which = iota((1, HD), 1) % half
    inv = jnp.ones((1, HD), F32)
    for j in range(1, half):
        inv = jnp.where(which == j, np.float32(10000.0 ** (-j / half)), inv)
    angle = (me * tokens + iota((tokens, HD), 0)).astype(F32) * inv
    cosine[...] = jnp.cos(angle)
    wave = jnp.sin(angle)
    sine[...] = jnp.where(iota((tokens, HD), 1) < HD // 2, -wave, wave)
    loads[0].wait()
    live = jnp.where(chosen[...] >= 0, 1.0, 0.0).astype(BF16)
    spread = jnp.where(
        iota((count + 1, far.shape[0]), 0) == iota((count + 1, far.shape[0]), 1) // BLK + 1, 1.0, 0.0
    ).astype(BF16)
    rows_of = jnp.where(
        iota((tokens, blocks), 0) // BLK == iota((tokens, blocks), 1), 1.0, 0.0
    ).astype(BF16)
    lists = lax.dot_general(
        rows_of, live, (((1,), (1,)), ((), ())), preferred_element_type=F32
    ).astype(BF16)
    admitted = jnp.dot(lists, spread, preferred_element_type=F32)
    bias[...] = jnp.where(admitted > 0.5, 0.0, -jnp.inf)

    pl.semaphore_wait(barrier, expected)
    for k in range(count):
        @pl.when(me >= reaches[k])
        def _():
            request_copy(k).start()

        @pl.when(me < reaches[k])
        def _():
            far[k * BLK:(k + 1) * BLK, :] = jnp.zeros((BLK, far.shape[1]), BF16)

    if far.shape[0] > count * BLK:
        far[count * BLK:, :] = jnp.zeros((far.shape[0] - count * BLK, far.shape[1]), BF16)

    loads[4].start()
    loads[5].start()

    def project(weights, columns, rows=slice(None)):
        return jnp.dot(x[rows, :], weights[:, columns], preferred_element_type=F32)

    def rotated(t, rows=slice(None)):
        turned = pltpu.roll(t, HD // 2, 1)
        return (t * cosine[rows, :] + turned * sine[rows, :]).astype(BF16)

    loads[1].wait()
    loads[2].wait()
    t = project(wk, slice(0, kv_heads * HD))
    for h in range(kv_heads):
        kv[:, h * HD:(h + 1) * HD] = rotated(t[:, h * HD:(h + 1) * HD])
    loads[3].wait()
    kv[:, kv_heads * HD:] = project(wv, slice(0, kv_heads * HD)).astype(BF16)

    for k in range(count):
        span = slice(k * BLK, (k + 1) * BLK)

        @pl.when(me + reaches[k] < peers)
        def _():
            request_copy(k).wait_recv()
            asked = request[k][k + 1:k + 2, blocks - 1:blocks]
            inner = jnp.maximum(asked - me * blocks, 0) * BLK
            wanted = iota((BLK, tokens), 1) == iota((BLK, tokens), 0) + inner
            pick[span, :] = jnp.where(wanted, 1.0, 0.0).astype(BF16)

        @pl.when(me + reaches[k] >= peers)
        def _():
            pick[span, :] = jnp.zeros((BLK, tokens), BF16)

    stage[...] = jnp.dot(pick[...], kv[...], preferred_element_type=F32).astype(BF16)
    for k in range(count):
        @pl.when(me + reaches[k] < peers)
        def _():
            far_copy(k).start()

    loads[4].wait()

    def make_queries(rows):
        for first in range(0, heads, 2):
            t = project(wq, slice(first * HD, (first + 2) * HD), rows)
            for h in range(2):
                q[rows, (first + h) * HD:(first + h + 1) * HD] = rotated(
                    t[:, h * HD:(h + 1) * HD], rows
                )

    make_queries(slice(0, tokens // 2))

    for k in range(count):
        @pl.when(me >= reaches[k])
        def _():
            request_copy(k).wait_send()
            far_copy(k).wait_recv()

    def side_copy(i):
        rows = pl.ds(pl.multiple_of(i * TILE, TILE), TILE)
        return pltpu.make_async_remote_copy(
            src_ref=gathered.at[lane, rows], dst_ref=gathered.at[lane, rows],
            send_sem=side_send.at[i], recv_sem=side_recv.at[i],
            device_id=(me, partner), device_id_type=MESH,
        )

    def ring_copy(step, i):
        rows = pl.ds(pl.multiple_of(i * TILE, TILE), TILE)
        return pltpu.make_async_remote_copy(
            src_ref=gathered.at[lane, rows], dst_ref=gathered.at[lane, rows],
            send_sem=ring_send.at[step - 1, i], recv_sem=ring_recv.at[step - 1, i],
            device_id=(me, lax.rem(chip + step, chips) * 2 + core), device_id_type=MESH,
        )

    def origin(step):
        return lax.rem(chip - step + chips, chips)

    def pass_copy(step, i):
        rows = pl.ds(pl.multiple_of(i * TILE, TILE), TILE)
        slot = origin(step) * 2 + core
        return pltpu.make_async_remote_copy(
            src_ref=gathered.at[slot, rows], dst_ref=gathered.at[slot, rows],
            send_sem=pass_send.at[step - 1, i], recv_sem=pass_recv.at[step - 1, i],
            device_id=(me, partner), device_id_type=MESH,
        )

    row_id, col_id = iota((TILE, TILE), 0), iota((TILE, TILE), 1)
    near_bias = jnp.where((row_id // BLK == col_id // BLK) & (col_id <= row_id), 0.0, -jnp.inf)
    contract = (((1,), (1,)), ((), ()))

    def attend(i, carry):
        rows = pl.ds(pl.multiple_of(i * TILE, TILE), TILE)
        far_bias = bias[rows, :]
        logs = jnp.zeros((TILE, TILE), F32)
        for h in range(heads):
            g = h // group
            keys = slice(g * HD, (g + 1) * HD)
            vals = slice((kv_heads + g) * HD, (kv_heads + g + 1) * HD)
            qh = q[rows, h * HD:(h + 1) * HD]
            s_far = lax.dot_general(qh, far[:, keys], contract, preferred_element_type=F32)
            s_near = lax.dot_general(qh, kv[rows, keys], contract, preferred_element_type=F32)
            s_far = s_far * scale + far_bias
            s_near = s_near * scale + near_bias
            top = jnp.maximum(
                jnp.max(s_far, axis=1, keepdims=True), jnp.max(s_near, axis=1, keepdims=True)
            )
            p_far = jnp.exp(s_far - top)
            p_near = jnp.exp(s_near - top)
            total = jnp.sum(p_far, axis=1, keepdims=True) + jnp.sum(p_near, axis=1, keepdims=True)
            summed = jnp.dot(p_far.astype(BF16), far[:, vals], preferred_element_type=F32)
            summed += jnp.dot(p_near.astype(BF16), kv[rows, vals], preferred_element_type=F32)
            gathered[lane, rows, h * HD:(h + 1) * HD] = (summed / total).astype(BF16)
            logs = jnp.where(col_id == h, top + jnp.log(total), logs)
        log_total[:, rows] = jnp.transpose(logs)[:heads]
        for step in range(1, chips):
            ring_copy(step, i).start()
        side_copy(i).start()
        return carry

    lax.fori_loop(0, tiles // 2, attend, 0)
    make_queries(slice(tokens // 2, tokens))
    lax.fori_loop(tiles // 2, tiles, attend, 0)

    log_copy = pltpu.make_async_copy(log_total, log_hbm, store_sem.at[tiles])
    log_copy.start()

    def out_copy(i):
        rows = pl.ds(pl.multiple_of(i * TILE, TILE), TILE)
        return pltpu.make_async_copy(out.at[rows], out_hbm.at[rows], store_sem.at[i])

    width = heads * HD

    def term(slot, rows):
        return jnp.dot(
            gathered[slot, rows, :], wo[pl.ds(pl.multiple_of(slot * width, width), width), :],
            preferred_element_type=F32,
        )

    everything = pl.ds(0, tokens)
    loads[5].wait()
    acc[...] = term(lane, everything)

    def take_side(i, carry):
        side_copy(i).wait_recv()
        return carry

    lax.fori_loop(0, tiles, take_side, 0)
    acc[...] += term(partner, everything)

    def finish(i, carry):
        rows = pl.ds(pl.multiple_of(i * TILE, TILE), TILE)
        total = acc[rows, :]
        for step in range(1, chips):
            ring_copy(step, i).wait_recv()
            pass_copy(step, i).start()
            total += term(origin(step) * 2 + core, rows)
        for step in range(1, chips):
            pass_copy(step, i).wait_recv()
            total += term(origin(step) * 2 + 1 - core, rows)
        out[rows, :] = total.astype(BF16)
        out_copy(i).start()
        return carry

    lax.fori_loop(0, tiles, finish, 0)

    def drain(i, carry):
        side_copy(i).wait_send()
        out_copy(i).wait()
        for step in range(1, chips):
            ring_copy(step, i).wait_send()
            pass_copy(step, i).wait_send()
        return carry

    lax.fori_loop(0, tiles, drain, 0)
    log_copy.wait()
    for k in range(count):
        @pl.when(me + reaches[k] < peers)
        def _():
            far_copy(k).wait_send()


def local(peers, tp, inputs, w_query, w_key, w_value, w_out, chosen):
    tokens, _ = inputs.shape
    heads = w_query.shape[1] // HD
    kv_heads = w_key.shape[1] // HD
    chosen = chosen.T
    count = chosen.shape[0] - 1
    far_rows = -(-count * BLK // TILE) * TILE
    tiles = tokens // TILE
    chips = tp // 2
    hbm = pl.BlockSpec(memory_space=pltpu.HBM)
    dma = pltpu.SemaphoreType.DMA
    shapes = (
        jax.ShapeDtypeStruct((tokens, w_out.shape[1]), BF16),
        jax.ShapeDtypeStruct((heads, tokens), F32),
    )
    return pl.pallas_call(
        functools.partial(kernel, peers, tp),
        out_shape=shapes,
        in_specs=[hbm] * 6,
        out_specs=(hbm, hbm),
        scratch_shapes=[
            pltpu.VMEM(inputs.shape, BF16),
            pltpu.VMEM(w_query.shape, BF16),
            pltpu.VMEM(w_key.shape, BF16),
            pltpu.VMEM(w_value.shape, BF16),
            pltpu.VMEM(w_out.shape, BF16),
            pltpu.VMEM(chosen.shape, jnp.int32),
            pltpu.VMEM((tokens, HD), F32),
            pltpu.VMEM((tokens, HD), F32),
            pltpu.VMEM((tokens, 2 * kv_heads * HD), BF16),
            pltpu.VMEM((tokens, heads * HD), BF16),
            pltpu.VMEM((count,) + chosen.shape, jnp.int32),
            pltpu.VMEM((count * BLK, tokens), BF16),
            pltpu.VMEM((count * BLK, 2 * kv_heads * HD), BF16),
            pltpu.VMEM((far_rows, 2 * kv_heads * HD), BF16),
            pltpu.VMEM((tokens, far_rows), F32),
            pltpu.VMEM((tp, tokens, heads * HD), BF16),
            pltpu.VMEM((tokens, w_out.shape[1]), F32),
            pltpu.VMEM((tokens, w_out.shape[1]), BF16),
            pltpu.VMEM((heads, tokens), F32),
            dma((6,)), dma((tiles + 1,)),
            dma((count,)), dma((count,)), dma((count,)), dma((count,)),
            dma((chips - 1, tiles)), dma((chips - 1, tiles)),
            dma((tiles,)), dma((tiles,)),
            dma((chips - 1, tiles)), dma((chips - 1, tiles)),
        ],
        compiler_params=pltpu.CompilerParams(
            collective_id=0, has_side_effects=True, vmem_limit_bytes=66_000_000
        ),
    )(inputs, w_query, w_key, w_value, w_out, chosen)


def solution(mesh):
    placed = (
        P("kv", None),
        P(None, "tp"),
        P(None, "tp"),
        P(None, "tp"),
        P(None, "tp"),
        P("kv", None),
    )
    return jax.shard_map(
        functools.partial(local, mesh.shape["kv"], mesh.shape["tp"]),
        mesh=mesh, in_specs=placed, out_specs=(P("kv", "tp"), P("tp", "kv")), check_vma=False,
    )
```

profile of v0, /device:TPU:29, one launch (start us, length us, event | category | flops | bytes accessed | tf_op | source)
XLA Modules:
  0.0 33.4 jit_solution(348523722186868352)
XLA Ops:
  0.6 29.6 %shard_map.77 = (bf16[512,512]{1,0:T(8,128)(2,1)}, f32[4,512]{1,0:T(4,128)}) custom-call(bf16[512,2048]{1,0:T(8,128)(2,1)} %x_hbm.1, bf16[2048,512]{1,0:T(8,128)(2,1)} %wq_hbm.1, bf16[2048,256]{1,0:T(8,128)(2,1)} %wk_hbm.1, bf16[2048,256]{1,0:T(8,128)(2,1)} %wv_hbm.1, bf16[2048,512]{1,0:T(8,128)(2,1)} %wo_hbm.1, s32[8,16]{1,0:T(8,128)} %bitcast.1), custom_call_target="tpu_custom_call" | custom-call | tf_op jit(solution)/shard_map/pallas_call | solution.py:316
  30.2 1.9 %copy.10 = bf16[512,512]{1,0:T(8,128)(2,1)} copy(bf16[512,512]{1,0:T(8,128)(2,1)} %get-tuple-element.4) | data formatting | bytes 1048576
  32.1 1.3 %copy.11 = f32[4,512]{1,0:T(4,128)} copy(f32[4,512]{1,0:T(4,128)} %get-tuple-element.5) | data formatting | bytes 16384
where the time goes:
time: 33.6 us; the launch traced here: 33.4 us
  Pallas kernels  29.6 us (88%)
  local copies, waits for them, and re-layouts  3.16 us (9%)
  between operations  0.64 us (2%)
    pallas_call x1, Pallas kernels, local(): pl.pallas_call(functools.partial(kernel, peers, tp), out_shape=shapes, in...  29.6 us
    unnamed x2, local copies, waits for them, and re-layouts  3.16 us

commit v1 on v0

--- a/solution.py
+++ b/solution.py
@@ -22,9 +22,9 @@
 
 def kernel(
     peers, tp, x_hbm, wq_hbm, wk_hbm, wv_hbm, wo_hbm, chosen_hbm,
-    out_hbm, log_hbm,
-    x, wq, wk, wv, wo, chosen, cosine, sine, kv, q, request, pick, stage, far, bias, gathered, acc, out, log_total,
-    load_sem, store_sem, req_send, req_recv, far_send, far_recv,
+    out, log_total,
+    x, wq, wk, wv, wo, chosen, cosine, sine, kv, q, request, pick, stage, far, bias, gathered, acc,
+    load_sem, req_send, req_recv, far_send, far_recv,
     ring_send, ring_recv, side_send, side_recv, pass_send, pass_recv,
 ):
     tokens = x.shape[0]
@@ -240,13 +240,6 @@
     make_queries(slice(tokens // 2, tokens))
     lax.fori_loop(tiles // 2, tiles, attend, 0)
 
-    log_copy = pltpu.make_async_copy(log_total, log_hbm, store_sem.at[tiles])
-    log_copy.start()
-
-    def out_copy(i):
-        rows = pl.ds(pl.multiple_of(i * TILE, TILE), TILE)
-        return pltpu.make_async_copy(out.at[rows], out_hbm.at[rows], store_sem.at[i])
-
     width = heads * HD
 
     def term(slot, rows):
@@ -277,21 +270,18 @@
             pass_copy(step, i).wait_recv()
             total += term(origin(step) * 2 + 1 - core, rows)
         out[rows, :] = total.astype(BF16)
-        out_copy(i).start()
         return carry
 
     lax.fori_loop(0, tiles, finish, 0)
 
     def drain(i, carry):
         side_copy(i).wait_send()
-        out_copy(i).wait()
         for step in range(1, chips):
             ring_copy(step, i).wait_send()
             pass_copy(step, i).wait_send()
         return carry
 
     lax.fori_loop(0, tiles, drain, 0)
-    log_copy.wait()
     for k in range(count):
         @pl.when(me + reaches[k] < peers)
         def _():
@@ -308,16 +298,17 @@
     tiles = tokens // TILE
     chips = tp // 2
     hbm = pl.BlockSpec(memory_space=pltpu.HBM)
+    vmem = pl.BlockSpec(memory_space=pltpu.VMEM)
     dma = pltpu.SemaphoreType.DMA
     shapes = (
-        jax.ShapeDtypeStruct((tokens, w_out.shape[1]), BF16),
-        jax.ShapeDtypeStruct((heads, tokens), F32),
+        pltpu.VMEM((tokens, w_out.shape[1]), BF16),
+        pltpu.VMEM((heads, tokens), F32),
     )
     return pl.pallas_call(
         functools.partial(kernel, peers, tp),
         out_shape=shapes,
         in_specs=[hbm] * 6,
-        out_specs=(hbm, hbm),
+        out_specs=(vmem, vmem),
         scratch_shapes=[
             pltpu.VMEM(inputs.shape, BF16),
             pltpu.VMEM(w_query.shape, BF16),
@@ -336,16 +327,14 @@
             pltpu.VMEM((tokens, far_rows), F32),
             pltpu.VMEM((tp, tokens, heads * HD), BF16),
             pltpu.VMEM((tokens, w_out.shape[1]), F32),
-            pltpu.VMEM((tokens, w_out.shape[1]), BF16),
-            pltpu.VMEM((heads, tokens), F32),
-            dma((6,)), dma((tiles + 1,)),
+            dma((6,)),
             dma((count,)), dma((count,)), dma((count,)), dma((count,)),
             dma((chips - 1, tiles)), dma((chips - 1, tiles)),
             dma((tiles,)), dma((tiles,)),
             dma((chips - 1, tiles)), dma((chips - 1, tiles)),
         ],
         compiler_params=pltpu.CompilerParams(
-            collective_id=0, has_side_effects=True, vmem_limit_bytes=66_000_000
+            collective_id=0, has_side_effects=True, vmem_limit_bytes=66_400_000
         ),
     )(inputs, w_query, w_key, w_value, w_out, chosen)
 

time: 33.6 us -> 31.1 us (0.926)
  local copies, waits for them, and re-layouts: 3.16 us -> 1.39 us
  Pallas kernels: 29.6 us -> 28.9 us
    unnamed x2, local copies, waits for them, and re-layouts: 3.16 us -> 1.39 us
    pallas_call x1, Pallas kernels: 29.6 us -> 28.9 us  [local(): pl.pallas_call(functools.partial(kernel, peers, tp), out_shape=shapes, in...]
where the time goes in v1:
time: 31.1 us; the launch traced here: 30.9 us
  Pallas kernels  28.9 us (93%)
  local copies, waits for them, and re-layouts  1.39 us (4%)
  between operations  0.64 us (2%)
    pallas_call x1, Pallas kernels, local(): pl.pallas_call(functools.partial(kernel, peers, tp), out_shape=shapes, in...  28.9 us
    unnamed x2, local copies, waits for them, and re-layouts  1.39 us

profile of v1, /device:TPU:29, one launch (start us, length us, event | category | flops | bytes accessed | tf_op | source)
XLA Modules:
  0.0 30.9 jit_solution(14884380910497673488)
XLA Ops:
  0.6 28.9 %shard_map.77 = (bf16[512,512]{1,0:T(8,128)(2,1)S(1)}, f32[4,512]{1,0:T(4,128)S(1)}) custom-call(bf16[512,2048]{1,0:T(8,128)(2,1)} %x_hbm.1, bf16[2048,512]{1,0:T(8,128)(2,1)} %wq_hbm.1, bf16[2048,256]{1,0:T(8,128)(2,1)} %wk_hbm.1, bf16[2048,256]{1,0:T(8,128)(2,1)} %wv_hbm.1, bf16[2048,512]{1,0:T(8,128)(2,1)} %wo_hbm.1, s32[8,16]{1,0:T(8,128)} %bitcast.1), custom_call_target="tpu_custom_call" | custom-call | tf_op jit(solution)/shard_map/pallas_call | solution.py:307
  29.6 0.8 %copy.10 = bf16[512,512]{1,0:T(8,128)(2,1)} copy(bf16[512,512]{1,0:T(8,128)(2,1)S(1)} %get-tuple-element.2) | data formatting | bytes 1048576
  30.3 0.6 %copy.11 = f32[4,512]{1,0:T(4,128)} copy(f32[4,512]{1,0:T(4,128)S(1)} %get-tuple-element.3) | data formatting | bytes 16384

commit v2 on v1

v2 whole, which is shorter than its diff:
```python
import contextlib
import functools

import jax
import jax.numpy as jnp
import numpy as np
from jax import lax
from jax.experimental import pallas as pl
from jax.experimental.pallas import tpu as pltpu
from jax.sharding import PartitionSpec as P

HD = 128
BLK = 32
TILE = 128
MESH = pl.DeviceIdType.MESH
F32 = jnp.float32
BF16 = jnp.bfloat16
LOG2E = 1.4426950408889634


def scope(name):
    return contextlib.nullcontext()


def iota(shape, dim):
    return lax.broadcasted_iota(jnp.int32, shape, dim)


def kernel(
    peers, tp, x_hbm, wq_hbm, wk_hbm, wv_hbm, wo_hbm, chosen_hbm,
    out, log_total,
    x, wq, wkv, wo, chosen, cosine, sine, kv, q, request, stage, far, bias, gathered, acc,
    near_o, near_m,
    load_sem, req_send, req_recv, far_send, far_recv,
    ring_send, ring_recv, side_send, side_recv, pass_send, pass_recv,
):
    tokens = x.shape[0]
    heads = wq.shape[1] // HD
    kv_heads = wkv.shape[1] // (2 * HD)
    kv_wide = kv_heads * HD
    group = heads // kv_heads
    wide = group * HD
    blocks = tokens // BLK
    count = chosen.shape[0] - 1
    reaches = [1 + k * (peers - 2) // (count - 1) for k in range(count)]
    chips = tp // 2
    tiles = tokens // TILE
    me = lax.axis_index("kv")
    lane = lax.axis_index("tp")
    chip, core = lane // 2, lane % 2
    partner = chip * 2 + 1 - core
    scale = HD ** -0.5
    factor = scale * LOG2E

    loads = [
        pltpu.make_async_copy(s, d, load_sem.at[i])
        for i, (s, d) in enumerate(
            [(chosen_hbm, chosen), (x_hbm, x), (wk_hbm, wkv.at[:, pl.ds(0, kv_wide)]),
             (wv_hbm, wkv.at[:, pl.ds(kv_wide, kv_wide)]), (wq_hbm, wq), (wo_hbm, wo)]
        )
    ]
    barrier = pltpu.get_barrier_semaphore()
    pl.semaphore_signal(barrier, inc=1, device_id=(me, partner), device_id_type=MESH)
    for step in range(1, chips):
        other = lax.rem(chip + step, chips) * 2 + core
        pl.semaphore_signal(barrier, inc=1, device_id=(me, other), device_id_type=MESH)
    expected = jnp.int32(chips)
    for d in reaches:
        @pl.when(me + d < peers)
        def _():
            pl.semaphore_signal(barrier, inc=1, device_id=(me + d, lane), device_id_type=MESH)

        expected = expected + jnp.where(me >= d, 1, 0)
    for load in loads[:4]:
        load.start()

    def request_copy(k):
        return pltpu.make_async_remote_copy(
            src_ref=chosen, dst_ref=request.at[k], send_sem=req_send.at[k],
            recv_sem=req_recv.at[k], device_id=(me - reaches[k], lane), device_id_type=MESH,
        )

    def far_copy(k, g):
        rows, cols = pl.ds(k * BLK, BLK), pl.ds(g * 2 * HD, 2 * HD)
        return pltpu.make_async_remote_copy(
            src_ref=stage.at[rows, cols], dst_ref=far.at[rows, cols], send_sem=far_send.at[k, g],
            recv_sem=far_recv.at[k, g], device_id=(me + reaches[k], lane), device_id_type=MESH,
        )

    with scope("trig"):
        half = HD // 2
        fold = tokens // 2
        which = iota((1, HD), 1) % half
        inv = jnp.ones((1, HD), F32)
        for j in range(1, half):
            inv = jnp.where(which == j, np.float32(10000.0 ** (-j / half)), inv)
        low = iota((fold, HD), 1) < half
        position = me * tokens + iota((fold, HD), 0) + jnp.where(low, 0, fold)
        angle = position.astype(F32) * inv
        wave = jnp.cos(angle)
        turned = pltpu.roll(wave, half, 1)
        cosine[:fold, :] = jnp.where(low, wave, turned)
        cosine[fold:, :] = jnp.where(low, turned, wave)
        wave = jnp.sin(angle)
        turned = pltpu.roll(wave, half, 1)
        sine[:fold, :] = jnp.where(low, -wave, turned)
        sine[fold:, :] = jnp.where(low, -turned, wave)

    with scope("barr"):
        loads[0].wait()
        pl.semaphore_wait(barrier, expected)
    for k in range(count):
        @pl.when(me >= reaches[k])
        def _():
            request_copy(k).start()

        @pl.when(me < reaches[k])
        def _():
            far[k * BLK:(k + 1) * BLK, :] = jnp.zeros((BLK, far.shape[1]), BF16)

    if far.shape[0] > count * BLK:
        far[count * BLK:, :] = jnp.zeros((far.shape[0] - count * BLK, far.shape[1]), BF16)

    with scope("bias"):
        live = jnp.where(chosen[...] >= 0, 1.0, 0.0).astype(BF16)
        spread = jnp.where(
            iota((count + 1, far.shape[0]), 0) == iota((count + 1, far.shape[0]), 1) // BLK + 1, 1.0, 0.0
        ).astype(BF16)
        rows_of = jnp.where(
            iota((tokens, blocks), 0) // BLK == iota((tokens, blocks), 1), 1.0, 0.0
        ).astype(BF16)
        lists = lax.dot_general(
            rows_of, live, (((1,), (1,)), ((), ())), preferred_element_type=F32
        ).astype(BF16)
        admitted = jnp.dot(lists, spread, preferred_element_type=F32)
        bias[...] = jnp.where(admitted > 0.5, 0.0, -jnp.inf)

    def rotated(t, rows=slice(None)):
        turned = pltpu.roll(t, HD // 2, 1)
        return (t * cosine[rows, :] + turned * sine[rows, :]).astype(BF16)

    with scope("waitx"):
        loads[1].wait()
        loads[2].wait()
        loads[3].wait()
    loads[4].start()
    with scope("kvproj"):
        t = jnp.dot(x[...], wkv[...], preferred_element_type=F32)
        for h in range(kv_heads):
            at = 2 * h * HD
            kv[:, at:at + HD] = rotated(t[:, h * HD:(h + 1) * HD])
            kv[:, at + HD:at + 2 * HD] = t[:, kv_wide + h * HD:kv_wide + (h + 1) * HD].astype(BF16)
    loads[5].start()

    def serve(k):
        @pl.when(me + reaches[k] < peers)
        def _():
            request_copy(k).wait_recv()
            asked = jnp.broadcast_to(request[k, k + 1:k + 2, blocks - 1:blocks], (BLK, HD))
            chunks = [jnp.zeros((BLK, HD), BF16)] * (2 * kv_heads)
            for b in range(blocks):
                wanted = jnp.where(asked == me * blocks + b, 1.0, 0.0).astype(BF16)
                for c in range(2 * kv_heads):
                    chunks[c] += wanted * kv[b * BLK:(b + 1) * BLK, c * HD:(c + 1) * HD]
            for c in range(2 * kv_heads):
                stage[k * BLK:(k + 1) * BLK, c * HD:(c + 1) * HD] = chunks[c]
            far_copy(k, 0).start()

    def follow(k):
        @pl.when(me + reaches[k] < peers)
        def _():
            for g in range(1, kv_heads):
                far_copy(k, g).start()

    contract = (((1,), (1,)), ((), ()))
    ones = jnp.ones((TILE, HD), BF16)

    def stacked(i, g):
        rows = slice(i * TILE, (i + 1) * TILE)
        return jnp.concatenate(
            [q[rows, h * HD:(h + 1) * HD] for h in range(g * group, (g + 1) * group)], axis=0
        )

    def near(several):
        pairs = [(i, g) for i in several for g in range(kv_heads)]
        row_id, col_id = iota((TILE, TILE), 0), iota((TILE, TILE), 1)
        seen = (row_id // BLK == col_id // BLK) & (col_id <= row_id)
        near_bias = jnp.where(seen, 0.0, -jnp.inf)
        near_bias = jnp.concatenate([near_bias] * group, axis=0)
        scores = []
        for i, g in pairs:
            keys = kv[i * TILE:(i + 1) * TILE, 2 * g * HD:(2 * g + 1) * HD]
            scores.append(lax.dot_general(stacked(i, g), keys, contract, preferred_element_type=F32))
        scores = [s + near_bias for s in scores]
        tops = [jnp.max(s, axis=1, keepdims=True) for s in scores]
        weights = [jnp.exp2((s - top) * factor).astype(BF16) for s, top in zip(scores, tops)]
        for (i, g), p, top in zip(pairs, weights, tops):
            at = (2 * g + 1) * HD
            vals = jnp.concatenate([kv[i * TILE:(i + 1) * TILE, at:at + HD], ones], axis=1)
            near_o[i, g] = jnp.dot(p, vals, preferred_element_type=F32)
            near_m[i, g] = jnp.broadcast_to(top, (group * TILE, HD))

    early = me >= reaches[0]

    def serve_if(when, some, after=()):
        @pl.when(when)
        def _():
            for k in some:
                if k < count:
                    serve(k)
            for k in after:
                if k < count:
                    follow(k)

    with scope("serve1"):
        serve_if(early, (0, 1))
    with scope("q"):
        loads[4].wait()
        t = jnp.dot(x[...], wq[...], preferred_element_type=F32)
        for h in range(heads):
            q[:, h * HD:(h + 1) * HD] = rotated(t[:, h * HD:(h + 1) * HD])
    with scope("serve2"):
        serve_if(early, (2, 3, 4), (0, 1))
    with scope("near1"):
        near(range(0, tiles // 2))
    with scope("serve3"):
        serve_if(early, (5,), (2, 3, 4))
    with scope("near2"):
        near(range(tiles // 2, tiles))
    with scope("serve4"):
        serve_if(early, range(6, count), range(5, count))
        serve_if(jnp.logical_not(early), (0, 1, 2))

    def await_far(g):
        for k in range(count):
            @pl.when(me >= reaches[k])
            def _():
                far_copy(k, g).wait_recv()

    def side_copy(i, g):
        rows = pl.ds(pl.multiple_of(i * TILE, TILE), TILE)
        cols = pl.ds(g * wide, wide)
        return pltpu.make_async_remote_copy(
            src_ref=gathered.at[lane, rows, cols], dst_ref=gathered.at[lane, rows, cols],
            send_sem=side_send.at[i, g], recv_sem=side_recv.at[i, g],
            device_id=(me, partner), device_id_type=MESH,
        )

    def ring_copy(step, i, g):
        rows = pl.ds(pl.multiple_of(i * TILE, TILE), TILE)
        cols = pl.ds(g * wide, wide)
        return pltpu.make_async_remote_copy(
            src_ref=gathered.at[lane, rows, cols], dst_ref=gathered.at[lane, rows, cols],
            send_sem=ring_send.at[step - 1, i, g], recv_sem=ring_recv.at[step - 1, i, g],
            device_id=(me, lax.rem(chip + step, chips) * 2 + core), device_id_type=MESH,
        )

    def origin(step):
        return lax.rem(chip - step + chips, chips)

    def pass_copy(step, i, g):
        rows = pl.ds(pl.multiple_of(i * TILE, TILE), TILE)
        cols = pl.ds(g * wide, wide)
        slot = origin(step) * 2 + core
        return pltpu.make_async_remote_copy(
            src_ref=gathered.at[slot, rows, cols], dst_ref=gathered.at[slot, rows, cols],
            send_sem=pass_send.at[step - 1, i, g], recv_sem=pass_recv.at[step - 1, i, g],
            device_id=(me, partner), device_id_type=MESH,
        )

    def attend(several, g):
        keys = far[:, 2 * g * HD:(2 * g + 1) * HD]
        vals = jnp.concatenate(
            [far[:, (2 * g + 1) * HD:(2 * g + 2) * HD], jnp.ones((far.shape[0], HD), BF16)], axis=1
        )
        scores = []
        for i in several:
            mask = jnp.concatenate([bias[i * TILE:(i + 1) * TILE, :]] * group, axis=0)
            s = lax.dot_general(stacked(i, g), keys, contract, preferred_element_type=F32)
            scores.append(s + mask)
        tops = [
            jnp.maximum(near_m[i, g], jnp.max(s, axis=1, keepdims=True))
            for i, s in zip(several, scores)
        ]
        weights = [
            jnp.concatenate([
                jnp.exp2((s[:, c:c + HD] - top) * factor).astype(BF16)
                for c in range(0, far.shape[0], HD)
            ], axis=1)
            for s, top in zip(scores, tops)
        ]
        for i, p, top in zip(several, weights, tops):
            rows = slice(i * TILE, (i + 1) * TILE)
            summed = jnp.dot(p, vals, preferred_element_type=F32)
            fade = jnp.exp2((near_m[i, g] - top) * factor)
            total = summed[:, HD:] + fade * near_o[i, g, :, HD:]
            done = summed[:, :HD] + fade * near_o[i, g, :, :HD]
            done = (done * (1.0 / total)).astype(BF16)
            for h in range(group):
                at = (g * group + h) * HD
                gathered[lane, rows, at:at + HD] = done[h * TILE:(h + 1) * TILE]
            for step in range(1, chips):
                ring_copy(step, i, g).start()
            side_copy(i, g).start()
            near_m[i, g] = top * scale + jnp.log(total)

    for g in range(kv_heads):
        with scope("waitfar"):
            await_far(g)
        for first in range(0, tiles, 2):
            with scope("att"):
                attend(range(first, first + 2), g)
            if g == 0 and first == 0:
                with scope("serve5"):
                    serve_if(jnp.logical_not(early), range(3, count), range(count))

    def logs():
        lane_id = iota((TILE, TILE), 1)
        for i in range(tiles):
            rows = jnp.zeros((TILE, TILE), F32)
            for h in range(heads):
                part = slice(h % group * TILE, (h % group + 1) * TILE)
                rows = jnp.where(lane_id == h, near_m[i, h // group, part, :], rows)
            log_total[:, i * TILE:(i + 1) * TILE] = jnp.transpose(rows)[:heads]

    width = heads * HD

    def term(slot, rows):
        return jnp.dot(
            gathered[slot, rows, :], wo[pl.ds(pl.multiple_of(slot * width, width), width), :],
            preferred_element_type=F32,
        )

    everything = pl.ds(0, tokens)
    with scope("ownterm"):
        loads[5].wait()
        acc[...] = term(lane, everything)

    with scope("logs"):
        logs()

    def part(slot, i, g):
        at = pl.multiple_of(slot * width + g * wide, wide)
        return jnp.dot(
            gathered[slot, i * TILE:(i + 1) * TILE, g * wide:(g + 1) * wide], wo[pl.ds(at, wide), :],
            preferred_element_type=F32,
        )

    with scope("waitside"):
        for i in range(tiles):
            for g in range(kv_heads):
                side_copy(i, g).wait_recv()
    with scope("sideterm"):
        acc[...] += term(partner, everything)

    pieces = [(i, g) for g in range(kv_heads) for i in range(tiles)]

    def finish(i, g):
        rows = slice(i * TILE, (i + 1) * TILE)
        with scope("waitpass"):
            for step in range(1, chips):
                pass_copy(step, i, g).wait_recv()
        total = acc[rows, :]
        for step in range(1, chips):
            total += part(origin(step) * 2 + 1 - core, i, g)
        if g == kv_heads - 1:
            out[rows, :] = total.astype(BF16)
        else:
            acc[rows, :] = total

    for n, (i, g) in enumerate(pieces):
        rows = slice(i * TILE, (i + 1) * TILE)
        with scope("waitring"):
            for step in range(1, chips):
                ring_copy(step, i, g).wait_recv()
                pass_copy(step, i, g).start()
        total = acc[rows, :]
        for step in range(1, chips):
            total += part(origin(step) * 2 + core, i, g)
        acc[rows, :] = total
        if n:
            finish(*pieces[n - 1])
    finish(*pieces[-1])

    def drain(i, carry):
        for g in range(kv_heads):
            side_copy(i, g).wait_send()
            for step in range(1, chips):
                ring_copy(step, i, g).wait_send()
                pass_copy(step, i, g).wait_send()
        return carry

    with scope("drain"):
        lax.fori_loop(0, tiles, drain, 0)
        for k in range(count):
            @pl.when(me >= reaches[k])
            def _():
                request_copy(k).wait_send()

            @pl.when(me + reaches[k] < peers)
            def _():
                for g in range(kv_heads):
                    far_copy(k, g).wait_send()


def local(peers, tp, inputs, w_query, w_key, w_value, w_out, chosen):
    tokens, _ = inputs.shape
    heads = w_query.shape[1] // HD
    kv_heads = w_key.shape[1] // HD
    chosen = chosen.T
    count = chosen.shape[0] - 1
    far_rows = -(-count * BLK // TILE) * TILE
    tiles = tokens // TILE
    chips = tp // 2
    hbm = pl.BlockSpec(memory_space=pltpu.HBM)
    vmem = pl.BlockSpec(memory_space=pltpu.VMEM)
    dma = pltpu.SemaphoreType.DMA
    shapes = (
        pltpu.VMEM((tokens, w_out.shape[1]), BF16),
        pltpu.VMEM((heads, tokens), F32),
    )
    return pl.pallas_call(
        functools.partial(kernel, peers, tp),
        out_shape=shapes,
        in_specs=[hbm] * 6,
        out_specs=(vmem, vmem),
        scratch_shapes=[
            pltpu.VMEM(inputs.shape, BF16),
            pltpu.VMEM(w_query.shape, BF16),
            pltpu.VMEM((w_key.shape[0], 2 * w_key.shape[1]), BF16),
            pltpu.VMEM(w_out.shape, BF16),
            pltpu.VMEM(chosen.shape, jnp.int32),
            pltpu.VMEM((tokens, HD), F32),
            pltpu.VMEM((tokens, HD), F32),
            pltpu.VMEM((tokens, 2 * kv_heads * HD), BF16),
            pltpu.VMEM((tokens, heads * HD), BF16),
            pltpu.VMEM((count,) + chosen.shape, jnp.int32),
            pltpu.VMEM((count * BLK, 2 * kv_heads * HD), BF16),
            pltpu.VMEM((far_rows, 2 * kv_heads * HD), BF16),
            pltpu.VMEM((tokens, far_rows), F32),
            pltpu.VMEM((tp, tokens, heads * HD), BF16),
            pltpu.VMEM((tokens, w_out.shape[1]), F32),
            pltpu.VMEM((tiles, kv_heads, heads // kv_heads * TILE, 2 * HD), F32),
            pltpu.VMEM((tiles, kv_heads, heads // kv_heads * TILE, HD), F32),
            dma((6,)),
            dma((count,)), dma((count,)), dma((count, kv_heads)), dma((count, kv_heads)),
            dma((chips - 1, tiles, kv_heads)), dma((chips - 1, tiles, kv_heads)),
            dma((tiles, kv_heads)), dma((tiles, kv_heads)),
            dma((chips - 1, tiles, kv_heads)), dma((chips - 1, tiles, kv_heads)),
        ],
        compiler_params=pltpu.CompilerParams(
            collective_id=0, has_side_effects=True, vmem_limit_bytes=66_400_000
        ),
    )(inputs, w_query, w_key, w_value, w_out, chosen)


def solution(mesh):
    placed = (
        P("kv", None),
        P(None, "tp"),
        P(None, "tp"),
        P(None, "tp"),
        P(None, "tp"),
        P("kv", None),
    )
    return jax.shard_map(
        functools.partial(local, mesh.shape["kv"], mesh.shape["tp"]),
        mesh=mesh, in_specs=placed, out_specs=(P("kv", "tp"), P("tp", "kv")), check_vma=False,
    )
```

time: 31.1 us -> 28.4 us (0.913)
  Pallas kernels: 28.9 us -> 26.1 us
    pallas_call x1, Pallas kernels: 28.9 us -> 26.1 us  [local(): pl.pallas_call(functools.partial(kernel, peers, tp), out_shape=shapes, in...]
where the time goes in v2:
time: 28.4 us; the launch traced here: 28.2 us
  Pallas kernels  26.1 us (92%)
  local copies, waits for them, and re-layouts  1.39 us (5%)
  between operations  0.64 us (2%)
    pallas_call x1, Pallas kernels, local(): pl.pallas_call(functools.partial(kernel, peers, tp), out_shape=shapes, in...  26.1 us
    unnamed x2, local copies, waits for them, and re-layouts  1.39 us

profile of v2, /device:TPU:29, one launch (start us, length us, event | category | flops | bytes accessed | tf_op | source)
XLA Modules:
  0.0 28.2 jit_solution(17691651951730805153)
XLA Ops:
  0.6 26.1 %shard_map.77 = (bf16[512,512]{1,0:T(8,128)(2,1)S(1)}, f32[4,512]{1,0:T(4,128)S(1)}) custom-call(bf16[512,2048]{1,0:T(8,128)(2,1)} %x_hbm.1, bf16[2048,512]{1,0:T(8,128)(2,1)} %wq_hbm.1, bf16[2048,256]{1,0:T(8,128)(2,1)} %wk_hbm.1, bf16[2048,256]{1,0:T(8,128)(2,1)} %wv_hbm.1, bf16[2048,512]{1,0:T(8,128)(2,1)} %wo_hbm.1, s32[8,16]{1,0:T(8,128)} %bitcast.1), custom_call_target="tpu_custom_call" | custom-call | tf_op jit(solution)/shard_map/pallas_call | solution.py:422
  26.8 0.8 %copy.10 = bf16[512,512]{1,0:T(8,128)(2,1)} copy(bf16[512,512]{1,0:T(8,128)(2,1)S(1)} %get-tuple-element.2) | data formatting | bytes 1048576
  27.6 0.6 %copy.11 = f32[4,512]{1,0:T(4,128)} copy(f32[4,512]{1,0:T(4,128)S(1)} %get-tuple-element.3) | data formatting | bytes 16384
